TPU v7x, 256 devices: a whole 4x4x8 slice. The times are simulated.
256 devices in a mesh: fs: 32 (over z, y), tp: 8 (over x, core).
Axes of the slice: x: 4, y: 4, z: 8, core: 2. Of those that a mesh axis runs over, the one named last changes fastest.
Arguments:
- stream: bfloat16 [12288, 2048], P('fs', 'tp'), may hold values from -3 to 3
- gain_first: float32 [2048], replicated, may hold values from 0.1 to 1.9
- gain_mixer: float32 [2048], replicated, may hold values from 0.1 to 1.9
- gain_second: float32 [2048], replicated, may hold values from 0.1 to 1.9
- gate_weight: float32 [2048, 5632], P('fs', 'tp'), may hold values from -0.125 to 0.125
- gate_scale: float32 [5632], P('tp'), may hold values from 0.5 to 2
- up_weight: float32 [2048, 5632], P('fs', 'tp'), may hold values from -0.125 to 0.125
- up_scale: float32 [5632], P('tp'), may hold values from 0.5 to 2
- down_weight: float32 [5632, 2048], P('tp', 'fs'), may hold values from -0.15625 to 0.15625
- down_scale: float32 [2048], P('tp'), may hold values from 0.5 to 2
- pool_in_weight: float32 [2048, 512], P('fs', 'tp'), may hold values from -0.125 to 0.125
- pool_in_scale: float32 [512], P('tp'), may hold values from 0.5 to 2
- pool_out_weight: float32 [512, 2048], P('tp', 'fs'), may hold values from -0.5 to 0.5
- pool_out_scale: float32 [2048], P('tp'), may hold values from 0.5 to 2
Outputs:
- layer_out: bfloat16 [12288, 2048], P('fs', 'tp')
All inputs are finite; a program needn't handle non-finite values.
Results may differ from a plain program's by a relative error of at most 0.025.
Values may be sent and summed in bfloat16 or wider, within the bound.
A program may use at most 64 MiB of HBM per device.

v0:
```python
import jax
import jax.numpy as jnp
from jax import lax
from jax.sharding import PartitionSpec as P

SEQ = 128


eps = 1e-06
WINDOWS = (2, 4, 8, 16)


def in_order(pieces, dim):
    pieces = jnp.moveaxis(pieces, 0, dim)
    lengths = pieces.shape
    return pieces.reshape(*lengths[:dim], lengths[dim] * lengths[dim + 1], *lengths[dim + 2 :])


def from_everyone(array, axis):
    copies = jnp.broadcast_to(array, (lax.axis_size(axis), *array.shape))
    return lax.all_to_all(copies, axis, split_axis=0, concat_axis=0, tiled=True)


def gathered_copies(array, axis, dim):
    return in_order(from_everyone(array, axis), dim)


def cut_along(array, dim, size):
    before, after = (array.shape[:dim], array.shape[dim + 1 :])
    return jnp.moveaxis(array.reshape(*before, size, -1, *after), dim, 0)


def sum_at_owner(array, axis, dim):
    size = lax.axis_size(axis)
    pieces = lax.all_to_all(cut_along(array, dim, size), axis, 0, 0, tiled=True)
    return jnp.sum(pieces.astype(jnp.float32), axis=0)


def gather_turned(arrays, axis, dims):
    turned = [jnp.moveaxis(a, dim, 0) for a, dim in zip(arrays, dims)]
    both = jnp.concatenate([t.reshape(len(t), -1) for t in turned], axis=1)
    whole, at, done = (lax.all_gather(both, axis, axis=0, tiled=True), 0, [])
    for t, dim in zip(turned, dims):
        piece = whole[:, at : at + t[0].size].reshape(-1, *t.shape[1:])
        done.append(jnp.moveaxis(piece, 0, dim))
        at += t[0].size
    return tuple(done)


def normed(own_columns, norm_gain):
    gathered = gathered_copies(own_columns, "tp", 1)
    floats = gathered.astype(jnp.float32)
    scaled = floats * lax.rsqrt(jnp.mean(floats * floats, axis=-1, keepdims=True) + eps)
    return (scaled * norm_gain).astype(jnp.bfloat16)


def residual_add(own_columns, partial_value, column_scale, factor):
    summed = sum_at_owner(partial_value.astype(jnp.bfloat16), "tp", 1)
    return (own_columns.astype(jnp.float32) + factor * (summed * column_scale)).astype(jnp.bfloat16)


def pooling(pool_input):
    channels = pool_input.shape[1]
    floats = pool_input.astype(jnp.float32).reshape(-1, SEQ, channels)
    csum = jnp.concatenate(
        [jnp.zeros((floats.shape[0], 1, channels), jnp.float32), jnp.cumsum(floats, axis=1)], axis=1
    )
    position = jnp.arange(SEQ)
    channel_index = lax.axis_index("tp") * channels + jnp.arange(channels, dtype=jnp.int32)
    channel_group = channel_index * 4 // (channels * lax.axis_size("tp"))
    pooled = -floats
    for group_index, window in enumerate(WINDOWS):
        before = window // 2
        after_span = window - before
        upper_sum = jnp.pad(csum, ((0, 0), (0, after_span), (0, 0)), mode="edge")[
            :, after_span : after_span + SEQ
        ]
        lower_sum = jnp.pad(csum, ((0, 0), (before, 0), (0, 0)), mode="edge")[:, :SEQ]
        counts = (
            jnp.minimum(position + after_span, SEQ) - jnp.maximum(position - before, 0)
        ).astype(jnp.float32)
        window_mean = (upper_sum - lower_sum) / counts[None, :, None]
        select = (channel_group == group_index).astype(jnp.float32)
        pooled = pooled + window_mean * select
    return pooled.reshape(-1, channels).astype(jnp.bfloat16)


def body(
    stream,
    gain_first,
    gain_mixer,
    gain_second,
    gate_weight,
    gate_scale,
    up_weight,
    up_scale,
    down_weight,
    down_scale,
    pool_in_weight,
    pool_in_scale,
    pool_out_weight,
    pool_out_scale,
):
    gate_half = gate_weight.astype(jnp.bfloat16)
    up_half = up_weight.astype(jnp.bfloat16)
    down_half = down_weight.astype(jnp.bfloat16)
    in_half = pool_in_weight.astype(jnp.bfloat16)
    out_half = pool_out_weight.astype(jnp.bfloat16)
    in_whole, out_whole = gather_turned((in_half, out_half), "fs", (0, 1))
    gate_whole, up_whole, down_whole = gather_turned(
        (gate_half, up_half, down_half), "fs", (0, 0, 1)
    )

    def feed_forward(normed_rows):
        gate_sum = jnp.dot(normed_rows, gate_whole, preferred_element_type=jnp.float32) * gate_scale
        up_sum = jnp.dot(normed_rows, up_whole, preferred_element_type=jnp.float32) * up_scale
        hidden = (jax.nn.silu(gate_sum) * up_sum).astype(jnp.bfloat16)
        return jnp.dot(hidden, down_whole, preferred_element_type=jnp.float32)

    after_first = residual_add(stream, feed_forward(normed(stream, gain_first)), down_scale, 0.5)
    mixer_normed = normed(after_first, gain_mixer)
    pool_input = (
        jnp.dot(mixer_normed, in_whole, preferred_element_type=jnp.float32) * pool_in_scale
    ).astype(jnp.bfloat16)
    pooled = pooling(pool_input)
    tp_count = lax.axis_size("tp")
    all_pooled = gathered_copies(pooled, "tp", 1)
    out_columns = lax.all_to_all(out_whole, "tp", split_axis=1, concat_axis=0, tiled=True)
    block_width = out_columns.shape[0] // tp_count
    pooled_blocks = all_pooled.reshape(all_pooled.shape[0], tp_count, block_width)
    weight_blocks = out_columns.reshape(tp_count, block_width, out_columns.shape[1])
    partials = jnp.einsum(
        "rbc,bcd->brd", pooled_blocks, weight_blocks, preferred_element_type=jnp.float32
    ).astype(jnp.bfloat16)
    mixed = jnp.sum(partials.astype(jnp.float32), axis=0)
    after_mix = (after_first.astype(jnp.float32) + mixed * pool_out_scale).astype(jnp.bfloat16)
    return residual_add(after_mix, feed_forward(normed(after_mix, gain_second)), down_scale, 0.5)


def solution(mesh):
    placed = (
        P("fs", "tp"),
        P(),
        P(),
        P(),
        P("fs", "tp"),
        P("tp"),
        P("fs", "tp"),
        P("tp"),
        P("tp", "fs"),
        P("tp"),
        P("fs", "tp"),
        P("tp"),
        P("tp", "fs"),
        P("tp"),
    )
    return jax.shard_map(body, mesh=mesh, in_specs=placed, out_specs=P("fs", "tp"), check_vma=False)
```

profile of v0, /device:TPU:1, one launch (start us, length us, event | category | flops | bytes accessed | tf_op | source)
XLA Modules:
  0.0 301.6 jit_solution(18422723841458305972)
XLA Ops:
  6.5 0.0 all-gather.2.cloned.1.call-start
  6.5 1.0 convert_bitcast_fusion
  7.5 0.9 convert_element_type.177
  8.5 0.9 convert_element_type.178
  9.4 0.9 concatenate.48
  10.3 0.0 all-gather.2.cloned.1.call-update
  10.3 0.0 copy-done
  10.3 0.2 copy.27
  10.5 0.1 broadcast_in_dim.15
  10.6 26.2 %all_to_all.46 = bf16[8,384,256]{1,2,0:T(8,128)(2,1)S(1)} all-to-all(bf16[8,384,256]{1,2,0:T(8,128)(2,1)S(1)} %broadcast_in_dim.15), channel_id=1, replica_groups=mesh['fs'=32,'tp'=8] {'tp'}, dimensions={0} | all-to-all | bytes 3145728 | tf_op jit(solution)/shard_map/all_to_all | solution.py:21
  36.8 0.4 multiply_reduce_fusion.2
  37.2 0.3 copy-done.3
  37.5 0.4 fusion.5
  37.9 0.0 copy-start.9
  37.9 76.1 %all-gather.2.cloned.1.call-done = bf16[2048,2112]{1,0:T(8,128)(2,1)} async-done(((bf16[64,2112]{1,0:T(8,128)(2,1)}), bf16[2048,2112]{1,0:T(8,128)(2,1)}) %all-gather.2.cloned.1.call-update) | async-done | bytes 8650768 | tf_op jit(solution)/shard_map/all_gather | solution.py:42
  114.0 0.0 copy-done.8
  114.0 4.7 %fusion.16 = f32[384,704]{0,1:T(8,128)} fusion(bf16[384,2048]{0,1:T(8,128)(2,1)S(1)} %fusion.5, bf16[2048,2112]{1,0:T(8,128)(2,1)} %all-gather.2.cloned.1.call-done, f32[704]{0:T(1024)S(1)} %copy-done.8), kind=kOutput, calls=%fused_computation.30 | convolution fusion | flops 1107566592 | bytes 5802752 | tf_op jit(solution)/shard_map/dot_general | solution.py:115
  118.7 0.0 copy-done.9
  118.7 7.7 %convolution_convert_fusion.1 = bf16[384,2048]{1,0:T(8,128)(2,1)S(1)} fusion(bf16[2048,2112]{1,0:T(8,128)(2,1)} %all-gather.2.cloned.1.call-done, bf16[384,2048]{0,1:T(8,128)(2,1)S(1)} %fusion.5, f32[384,704]{0,1:T(8,128)} %fusion.16, f32[704]{0:T(1024)S(1)} %copy-done.9), kind=kOutput, calls=%fused_computation.16 | convolution fusion | flops 2217271296 | bytes 10521344 | tf_op jit(solution)/shard_map/dot_general | solution.py:118
  126.4 0.1 copy.48
  126.5 26.0 %all_to_all.47 = bf16[8,384,256]{2,1,0:T(8,128)(2,1)S(1)} all-to-all(bf16[8,384,256]{2,1,0:T(8,128)(2,1)S(1)} %bitcast.62), channel_id=1, replica_groups=mesh['fs'=32,'tp'=8] {'tp'}, dimensions={0} | all-to-all | bytes 3145728 | tf_op jit(solution)/shard_map/all_to_all | solution.py:35
  152.5 0.2 convert_reduce_fusion.2
  152.8 0.5 copy-done.6
  153.2 0.1 add_convert_fusion.2
  153.3 0.2 copy.29
  153.5 1.3 broadcast_in_dim.17
  154.8 4.7 %all-to-all-start.2 = ((bf16[8,384,256]{1,2,0:T(8,128)(2,1)}), bf16[8,384,256]{1,2,0:T(8,128)(2,1)S(1)}, u32[]{:S(2)}, u32[]{:S(2)}) async-start(bf16[8,384,256]{1,2,0:T(8,128)(2,1)} %broadcast_in_dim.17), calls=%async_computation.2 | async-start | bytes 3145728 | tf_op jit(solution)/shard_map/all_to_all | solution.py:21
  159.4 0.0 copy-done.1
  159.4 0.1 copy.30
  159.5 0.0 copy-done.2
  159.5 0.1 pad_maximum_fusion.11
  159.6 37.7 %all_gather.7 = bf16[2048,128]{1,0:T(8,128)(2,1)S(1)} all-gather(bf16[64,128]{1,0:T(8,128)(2,1)S(1)} %pad_maximum_fusion.11), channel_id=1, replica_groups=mesh['fs'=32,'tp'=8] {'fs'}, dimensions={0}, use_global_device_ids=true | all-gather | bytes 540672 | tf_op jit(solution)/shard_map/all_gather | solution.py:42
  197.3 0.2 slice.86
  197.6 0.0 copy-start.4
  197.6 0.9 copy.35
  198.6 0.0 all-to-all-done.2
  198.6 14.6 %all-to-all-start.4 = ((bf16[64,8,256]{2,0,1:T(8,128)(2,1)}), bf16[64,8,256]{2,0,1:T(8,128)(2,1)S(1)}, u32[]{:S(2)}, u32[]{:S(2)}) async-start(bf16[64,8,256]{2,0,1:T(8,128)(2,1)} %copy.35), calls=%async_computation.4 | async-start | bytes 524288 | tf_op jit(solution)/shard_map/all_to_all | solution.py:128
  213.2 0.4 multiply_reduce_fusion.1
  213.7 0.0 copy-done.4
  213.7 0.0 copy-start.10
  213.7 0.4 fusion.3
  214.1 0.2 copy-done.10
  214.3 0.4 fusion.41
  214.7 0.1 copy.40
  214.9 0.2 reduce_window_sum.11
  215.1 0.0 copy-start.7
  215.1 0.3 fusion.75
  215.5 0.1 copy.33
  215.6 4.1 %all-to-all-done.4 = bf16[64,8,256]{2,0,1:T(8,128)(2,1)S(1)} async-done(((bf16[64,8,256]{2,0,1:T(8,128)(2,1)}), bf16[64,8,256]{2,0,1:T(8,128)(2,1)S(1)}, u32[]{:S(2)}, u32[]{:S(2)}) %all-to-all-start.4) | async-done | bytes 262176 | tf_op jit(solution)/shard_map/all_to_all | solution.py:128
  219.7 11.5 %all_to_all.48 = bf16[8,384,64]{1,2,0:T(8,128)(2,1)S(1)} all-to-all(bf16[8,384,64]{1,2,0:T(8,128)(2,1)S(1)} %broadcast_in_dim.18), channel_id=1, replica_groups=mesh['fs'=32,'tp'=8] {'tp'}, dimensions={0} | all-to-all | bytes 786432 | tf_op jit(solution)/shard_map/all_to_all | solution.py:21
  231.2 0.6 convert_reduce_fusion.1
  231.9 0.1 add_convert_fusion.1
  231.9 0.2 copy.36
  232.1 0.1 broadcast_in_dim.19
  232.2 23.9 %all_to_all.49 = bf16[8,384,256]{1,2,0:T(8,128)(2,1)S(1)} all-to-all(bf16[8,384,256]{1,2,0:T(8,128)(2,1)S(1)} %broadcast_in_dim.19), channel_id=1, replica_groups=mesh['fs'=32,'tp'=8] {'tp'}, dimensions={0} | all-to-all | bytes 3145728 | tf_op jit(solution)/shard_map/all_to_all | solution.py:21
  256.1 0.4 multiply_reduce_fusion
  256.5 0.3 copy-done.5
  256.8 0.4 fusion.1
  257.2 4.7 %fusion.19 = f32[384,704]{0,1:T(8,128)} fusion(bf16[384,2048]{0,1:T(8,128)(2,1)S(1)} %fusion.1, bf16[2048,2112]{1,0:T(8,128)(2,1)} %all-gather.2.cloned.1.call-done, f32[704]{0:T(1024)S(1)} %copy-done.8), kind=kOutput, calls=%fused_computation.31 | convolution fusion | flops 1107566592 | bytes 5802752 | tf_op jit(solution)/shard_map/dot_general | solution.py:115
  261.9 7.7 %convolution_convert_fusion = bf16[384,2048]{1,0:T(8,128)(2,1)S(1)} fusion(bf16[2048,2112]{1,0:T(8,128)(2,1)} %all-gather.2.cloned.1.call-done, bf16[384,2048]{0,1:T(8,128)(2,1)S(1)} %fusion.1, f32[384,704]{0,1:T(8,128)} %fusion.19, f32[704]{0:T(1024)S(1)} %copy-done.9), kind=kOutput, calls=%fused_computation.15 | convolution fusion | flops 2217271296 | bytes 10521344 | tf_op jit(solution)/shard_map/dot_general | solution.py:118
  269.6 0.1 copy.47
  269.7 24.0 %all_to_all.50 = bf16[8,384,256]{2,1,0:T(8,128)(2,1)S(1)} all-to-all(bf16[8,384,256]{2,1,0:T(8,128)(2,1)S(1)} %bitcast.63), channel_id=1, replica_groups=mesh['fs'=32,'tp'=8] {'tp'}, dimensions={0} | all-to-all | bytes 3145728 | tf_op jit(solution)/shard_map/all_to_all | solution.py:35
  293.8 0.2 convert_reduce_fusion
  294.0 0.7 add_convert_fusion
  (28 shorter events, 0.2 us)
Async XLA Ops:
  6.5 3.8 %copy-start = (bf16[384,256]{1,0:T(8,128)(2,1)S(1)}, bf16[384,256]{1,0:T(8,128)(2,1)}, u32[]{:S(2)}) copy-start(bf16[384,256]{1,0:T(8,128)(2,1)} %param.14) | copy-start | bytes 589828
  6.5 107.5 %all-gather.2.cloned.1.call-start = ((), (), s32[]{:S(2)}) async-start(), calls=%async_computation.7 | async-start | bytes 9191424 | tf_op jit(solution)/shard_map/all_gather | solution.py:42
  36.8 0.7 copy-start.3
  37.5 76.5 %copy-start.8 = (f32[704]{0:T(1024)S(1)}, f32[704]{0:T(1024)}, u32[]{:S(2)}) copy-start(f32[704]{0:T(1024)} %param.19) | copy-start | bytes 8452
  37.9 80.8 %copy-start.9 = (f32[704]{0:T(1024)S(1)}, f32[704]{0:T(1024)}, u32[]{:S(2)}) copy-start(f32[704]{0:T(1024)} %param.21) | copy-start | bytes 8452
  152.5 0.7 copy-start.6
  154.8 4.7 %copy-start.1 = (f32[64,64]{1,0:T(8,128)S(1)}, f32[64,64]{1,0:T(8,128)}, u32[]{:S(2)}) copy-start(f32[64,64]{1,0:T(8,128)} %param.26) | copy-start | bytes 49156
  154.8 4.7 %copy-start.2 = (f32[64,64]{1,0:T(8,128)S(1)}, f32[64,64]{1,0:T(8,128)}, u32[]{:S(2)}) copy-start(f32[64,64]{1,0:T(8,128)} %param.24) | copy-start | bytes 49156
  154.8 43.8 %all-to-all-start.2 = ((bf16[8,384,256]{1,2,0:T(8,128)(2,1)}), bf16[8,384,256]{1,2,0:T(8,128)(2,1)S(1)}, u32[]{:S(2)}, u32[]{:S(2)}) async-start(bf16[8,384,256]{1,2,0:T(8,128)(2,1)} %broadcast_in_dim.17), calls=%async_computation.2 | async-start | bytes 3145728 | tf_op jit(solution)/shard_map/all_to_all | solution.py:21
  197.6 16.1 %copy-start.4 = (f32[2048]{0:T(1024)S(1)}, f32[2048]{0:T(1024)}, u32[]{:S(2)}) copy-start(f32[2048]{0:T(1024)} %param.16) | copy-start | bytes 24580
  198.6 21.1 %all-to-all-start.4 = ((bf16[64,8,256]{2,0,1:T(8,128)(2,1)}), bf16[64,8,256]{2,0,1:T(8,128)(2,1)S(1)}, u32[]{:S(2)}, u32[]{:S(2)}) async-start(bf16[64,8,256]{2,0,1:T(8,128)(2,1)} %copy.35), calls=%async_computation.4 | async-start | bytes 524288 | tf_op jit(solution)/shard_map/all_to_all | solution.py:128
  213.7 0.7 copy-start.10
  215.1 16.7 %copy-start.7 = (f32[256]{0:T(256)S(1)}, f32[256]{0:T(256)}, u32[]{:S(2)}) copy-start(f32[256]{0:T(256)} %param.27) | copy-start | bytes 3076
  256.1 0.7 copy-start.5
Sparse Core Ops, SparseCore 0:
  10.4 103.5 all-gather.1
where the time goes:
time: 302 us
  blocking collectives  149 us (49%)
  waiting for transfers between devices  80.2 us (27%)
  matrix products  25.8 us (9%)
  starting transfers between devices  19.3 us (6%)
  between operations  13.7 us (5%)
  other arithmetic  7.36 us (2%)
  local copies, waits for them, and re-layouts  5.9 us (2%)
    all_gather x1, waiting for transfers between devices, gather_turned(): whole, at, done = (lax.all_gather(both, axis, axis=0, tiled=True), 0, [])  76.1 us
    all_to_all x3, blocking collectives, from_everyone(): return lax.all_to_all(copies, axis, split_axis=0, concat_axis=0, tiled=True)  61.5 us
    all_to_all x2, blocking collectives, sum_at_owner(): pieces = lax.all_to_all(cut_along(array, dim, size), axis, 0, 0, tiled=True)  50 us
    all_gather x1, blocking collectives, gather_turned(): whole, at, done = (lax.all_gather(both, axis, axis=0, tiled=True), 0, [])  37.7 us
    dot_general x2, matrix products, feed_forward(): return jnp.dot(hidden, down_whole, preferred_element_type=jnp.float32)  15.5 us
    all_to_all x1, starting transfers between devices, body(): lax.all_to_all(out_whole, 'tp', split_axis=1, concat_axis=0, tiled=True)  14.6 us
    dot_general x2, matrix products, feed_forward(): jnp.dot(normed_rows, gate_whole, preferred_element_type=jnp.float32)  9.33 us
  transfers between devices with their start and end apart: 3, of which 2 were waited for; matrix products, arithmetic and copies ran while one was open for 1% of the time, Pallas kernels for 0%

commit v1 on v0

v1 whole, which is shorter than its diff:
```python
import random

import jax
import jax.numpy as jnp
from jax import lax
from jax.experimental import pallas as pl
from jax.experimental.pallas import tpu as pltpu
from jax.sharding import PartitionSpec as P

SEQ = 128
EPS = 1e-06
WINDOWS = (2, 4, 8, 16)
NZ, NY, NX = 8, 4, 4
ROWS = 384
HALF = ROWS // 2
D = 2048
BLK = 256
FB = 704
GUW = 2 * FB
DH = FB // 2
BF = jnp.bfloat16
F32 = jnp.float32

SIZES = (0.36, 1, 1, 1, 1, 1, 1)
CLASSES = (0, 1, 1, 1, 1, 2, 2)
PIECES_G = (1, 2, 3, 4)
PIECES_D = (5, 6)


def moved(o, d):
    z, y = o
    if d == 0:
        return z, (y + 1) % NY
    if d == 1:
        return z, (y - 1) % NY
    return (z + (1 if d == 2 else -1)) % NZ, y


def broadcast_plan(lag=2.0, seed=43, noise=0.3):
    rng = random.Random(seed)
    count = len(SIZES)
    has = [{(0, 0): 0.0} for _ in range(count)]
    free = [0.0] * 4
    plan = []
    while len(plan) < count * (NZ * NY - 1):
        best = None
        for d in range(4):
            found = []
            for s in range(count):
                for o, t in has[s].items():
                    q = moved(o, d)
                    if q not in has[s]:
                        found.append((max(free[d], t), s, o, q))
            if found:
                first = min(c[0] for c in found)
                if best is None or first < best[0]:
                    best = (first, d, [c for c in found if c[0] <= first + 1e-9])
        _, d, found = best

        def key(c):
            onward = sum(moved(c[3], e) not in has[c[1]] for e in range(4))
            return CLASSES[c[1]], -noise * rng.random() * 4 - onward * 0.5 + len(has[c[1]]) * 0.02

        start, s, o, q = min(found, key=key)
        has[s][q] = start + SIZES[s] + lag
        free[d] = start + SIZES[s]
        plan.append((start, d, s, o))
    return plan, has


def kernel(
    stream, gain1, gainm, gain2, gw, gsc, uw, usc, dw, dsc, iw, isc, ow, osc,
    out,
    gbuf, dbuf, dfull, pall, sall, infull, outfull, xall1, xall2, nbuf, ambuf, hid, ssacc, rst, pacc, pooled,
    snd1, pre1, sr1, rr1, snd2, pre2, sr2, rr2, mine,
    psend, precv, a1s, a1r, a2s, a2r, pas, par, sas, sar, r1s, r1r, r2s, r2r,
):
    f, t = lax.axis_index("fs"), lax.axis_index("tp")
    z, y = f // NY, f % NY
    x, c = t // 2, t % 2
    oc = 1 - c

    def at_f(dz, dy):
        return ((z + dz + NZ) % NZ) * NY + (y + dy + NY) % NY

    def at_t(dx, core):
        return ((x + dx + NX) % NX) * 2 + core

    neighbour = [at_f(0, 1), at_f(0, -1), at_f(1, 0), at_f(-1, 0)]
    right, left, twin = at_t(1, c), at_t(-1, c), at_t(0, oc)

    barrier = pltpu.get_barrier_semaphore()
    for nf in neighbour:
        pl.semaphore_signal(barrier, inc=1, device_id={"fs": nf, "tp": t})
    for nt in (right, left, twin):
        pl.semaphore_signal(barrier, inc=1, device_id={"fs": f, "tp": nt})

    prow = pl.ds(pl.multiple_of(f * 64, 64), 64)
    pall[t, prow, :] = jnp.concatenate([iw[...], ow[...]], axis=1).astype(BF)
    for j in range(5):
        gbuf[prow, 256 * j : 256 * j + 128] = gw[:, 128 * j : 128 * j + 128].astype(BF)
        gbuf[prow, 256 * j + 128 : 256 * j + 256] = uw[:, 128 * j : 128 * j + 128].astype(BF)
    gbuf[prow, 1280:1408] = jnp.concatenate([gw[:, 640:704], uw[:, 640:704]], axis=1).astype(BF)
    dbuf[pl.ds(pl.multiple_of(f * DH, 32), DH), :] = jnp.concatenate([dw[0:DH, :], dw[DH:FB, :]], axis=1).astype(BF)
    xall1[t] = stream[...]
    sall[t] = jnp.concatenate(
        [jnp.broadcast_to(osc[...], (16, 256)), jnp.broadcast_to(isc[...], (16, 64)), jnp.zeros((16, 64), F32)], axis=1
    )
    pl.semaphore_wait(barrier, 7)

    def piece(s, owner):
        if s == 0:
            return pall.at[t, pl.ds(pl.multiple_of(owner * 64, 64), 64), :]
        if s in PIECES_G:
            return gbuf.at[pl.ds(pl.multiple_of(owner * 64 + 16 * (s - 1), 16), 16), :]
        return dbuf.at[pl.ds(pl.multiple_of(owner * DH + 176 * (s - 5), 16), 176), :]

    def owner_of(o):
        return at_f(-o[0], -o[1])

    arrived = set()

    def ensure(s, o):
        if o == (0, 0) or (s, o) in arrived:
            return
        arrived.add((s, o))
        ref = piece(s, owner_of(o))
        pltpu.make_async_remote_copy(
            src_ref=ref, dst_ref=ref, send_sem=psend.at[0], recv_sem=precv.at[s, o[0] * NY + o[1]],
            device_id={"fs": neighbour[0], "tp": t},
        ).wait_recv()

    def send_piece(d, s, o):
        ensure(s, o)
        q = moved(o, d)
        ref = piece(s, owner_of(o))
        pltpu.make_async_remote_copy(
            src_ref=ref, dst_ref=ref, send_sem=psend.at[0 if s == 0 else 1 if s in PIECES_G else 2],
            recv_sem=precv.at[s, q[0] * NY + q[1]], device_id={"fs": neighbour[d], "tp": t},
        ).start()

    class Ring:
        def __init__(self, part, whole, ssem, rsem):
            self.part, self.whole, self.ssem, self.rsem = part, whole, ssem, rsem

        def copy(self, ref, to, rs):
            return pltpu.make_async_remote_copy(
                src_ref=ref, dst_ref=ref, send_sem=self.ssem.at[1 if rs >= 6 else 0], recv_sem=self.rsem.at[rs],
                device_id={"fs": f, "tp": to},
            )

        def start(self):
            me = t
            self.copy(self.part(me, 0), right, 0).start()
            self.copy(self.part(me, 1), left, 3).start()
            self.copy(self.part(me, 1), right, 1).start()
            self.copy(self.part(me, 0), left, 2).start()
            self.copy(self.part(me, 0), twin, 6).start()
            self.copy(self.part(me, 1), twin, 7).start()

        def block(self, k, core):
            return at_t((-1, -1, 1, 1, 2, 2, 0, 0)[k], core), k % 2

        def got(self, k, share=True):
            ref = self.part(*self.block(k, c))
            self.copy(ref, twin, k).wait_recv()
            if k == 0:
                self.copy(ref, right, 4).start()
            if k == 3:
                self.copy(ref, left, 5).start()
            if share:
                self.copy(ref, twin, 8 + k).start()

        def got_twin(self, k):
            ref = self.part(*self.block(k, oc))
            self.copy(ref, twin, 8 + k if k < 6 else k).wait_recv()

        def done(self):
            pltpu.make_async_remote_copy(
                src_ref=self.whole(3), dst_ref=self.whole(3), send_sem=self.ssem.at[0], recv_sem=self.rsem.at[0],
                device_id={"fs": f, "tp": twin},
            ).wait_send()
            pltpu.make_async_remote_copy(
                src_ref=self.whole(4), dst_ref=self.whole(4), send_sem=self.ssem.at[1], recv_sem=self.rsem.at[0],
                device_id={"fs": f, "tp": twin},
            ).wait_send()

    def halves(buf, size):
        return (
            lambda b, h: buf.at[b, pl.ds(h * (size // 2), size // 2), :],
            lambda n: buf.at[pl.ds(0, n)],
        )

    ag1 = Ring(*halves(xall1, ROWS), a1s, a1r)
    ag2 = Ring(*halves(xall2, ROWS), a2s, a2r)
    pag = Ring(*halves(pall, D), pas, par)
    sag = Ring(*halves(sall, 16), sas, sar)
    sag.part = lambda b, h: sall.at[b, pl.ds(h * 8, 8), :]

    def norm_block(b, src, gain, first):
        v = src[b].astype(F32)
        sq = v * v
        sq = sq[:, :128] + sq[:, 128:]
        ssacc[...] = sq if first else ssacc[...] + sq
        return (v * gain[:, b * BLK : (b + 1) * BLK]).astype(BF)

    def finish_norm():
        mean = jnp.sum(ssacc[...], axis=1, keepdims=True) * (1.0 / D)
        rst[...] = jnp.broadcast_to(lax.rsqrt(mean + EPS), (ROWS, 128))

    def norm1(b):
        nbuf[:, b * BLK : (b + 1) * BLK] = norm_block(b, xall1, gain1, b == 0)

    def hidden(j):
        if j < 5:
            acc = jnp.dot(nbuf[...], gbuf[:, 256 * j : 256 * j + 256], preferred_element_type=F32)
            r = rst[...]
            g = acc[:, :128] * r * gsc[:, 128 * j : 128 * j + 128]
            u = acc[:, 128:] * r * usc[:, 128 * j : 128 * j + 128]
            hid[:, 128 * j : 128 * j + 128] = (g / (1.0 + jnp.exp(-g)) * u).astype(BF)
        else:
            acc = jnp.dot(nbuf[...], gbuf[:, 1280:1408], preferred_element_type=F32)
            scale = jnp.concatenate([gsc[:, 640:704], usc[:, 640:704]], axis=1)
            v = acc * rst[...] * scale
            u = pltpu.roll(v, 64, 1)
            h = v / (1.0 + jnp.exp(-v)) * u
            lane = lax.broadcasted_iota(jnp.int32, h.shape, 1)
            hid[:, 640:768] = jnp.where(lane < 64, h, 0.0).astype(BF)

    def unpack_down(b):
        for pair in range(2):
            one = dbuf[pl.ds(pl.multiple_of((4 * b + 2 * pair) * DH, 32), DH), :]
            two = dbuf[pl.ds(pl.multiple_of((4 * b + 2 * pair + 1) * DH, 32), DH), :]
            cols = slice(128 * pair, 128 * pair + 128)
            dfull[b, 0:DH, cols] = jnp.concatenate([one[:, :64], two[:, :64]], axis=1)
            dfull[b, DH:FB, cols] = jnp.concatenate([one[:, 64:], two[:, 64:]], axis=1)

    def unpack_in(k):
        rows = pl.ds(256 * k, 256)
        for i in range(NX):
            infull[rows, 128 * i : 128 * i + 128] = jnp.concatenate(
                [pall[2 * i, rows, :][:, :64], pall[2 * i + 1, rows, :][:, :64]], axis=1
            )

    def unpack_out(b):
        for i in range(16):
            outfull[64 * b : 64 * b + 64, 128 * i : 128 * i + 128] = jnp.concatenate(
                [pall[b, 128 * i : 128 * i + 64, :][:, 64:], pall[b, 128 * i + 64 : 128 * i + 128, :][:, 64:]], axis=1
            )

    def down(b):
        return jnp.dot(hid[...], dfull[b], preferred_element_type=F32)

    def summed_down(snd, pre, sr, rr, ss, rs):
        offs = (0, 1, 2, -1)
        A, B = pl.ds(0, HALF), pl.ds(HALF, HALF)

        def to_twin(k):
            snd[k] = down(at_t(offs[k], oc)).astype(BF)
            pltpu.make_async_remote_copy(
                src_ref=snd.at[k], dst_ref=pre.at[k], send_sem=ss.at[0], recv_sem=rs.at[k],
                device_id={"fs": f, "tp": twin},
            ).start()

        def own(k):
            mine[k] = down(at_t(offs[k], c))

        def both(k):
            pltpu.make_async_remote_copy(
                src_ref=snd.at[k], dst_ref=pre.at[k], send_sem=ss.at[0], recv_sem=rs.at[k],
                device_id={"fs": f, "tp": twin},
            ).wait_recv()

        def hop(src, slot, rows, sem, to):
            return pltpu.make_async_remote_copy(
                src_ref=src, dst_ref=rr.at[slot, rows, :], send_sem=ss.at[1], recv_sem=rs.at[sem],
                device_id={"fs": f, "tp": to},
            )

        to_twin(2)
        to_twin(1)
        own(2)
        both(2)
        sr[2] = (mine[2] + pre[2].astype(F32)).astype(BF)
        hop(sr.at[2, A, :], 2, A, 4, right).start()
        hop(sr.at[2, B, :], 2, B, 5, left).start()
        to_twin(3)
        own(1)
        both(1)
        sr[1, B, :] = (mine[1, B, :] + pre[1, B, :].astype(F32)).astype(BF)
        hop(sr.at[1, B, :], 0, B, 6, right).start()
        own(3)
        both(3)
        sr[0, A, :] = (mine[3, A, :] + pre[3, A, :].astype(F32)).astype(BF)
        hop(sr.at[0, A, :], 1, A, 7, left).start()
        to_twin(0)
        own(0)
        hop(sr.at[2, A, :], 2, A, 4, right).wait_recv()
        sr[1, A, :] = (mine[1, A, :] + pre[1, A, :].astype(F32) + rr[2, A, :].astype(F32)).astype(BF)
        hop(sr.at[1, A, :], 0, A, 8, right).start()
        hop(sr.at[2, B, :], 2, B, 5, left).wait_recv()
        sr[0, B, :] = (mine[3, B, :] + pre[3, B, :].astype(F32) + rr[2, B, :].astype(F32)).astype(BF)
        hop(sr.at[0, B, :], 1, B, 9, left).start()
        both(0)
        mine[0] = mine[0] + pre[0].astype(F32)
        hop(sr.at[1, B, :], 0, B, 6, right).wait_recv()
        hop(sr.at[0, A, :], 1, A, 7, left).wait_recv()
        hop(sr.at[1, A, :], 0, A, 8, right).wait_recv()
        hop(sr.at[0, B, :], 1, B, 9, left).wait_recv()
        mine[0] = mine[0] + rr[0].astype(F32) + rr[1].astype(F32)

    def summed_done(snd, sr, ss, rs):
        for ref, k in ((snd.at[pl.ds(0, 4)], 0), (sr.at[pl.ds(0, 3)], 1)):
            pltpu.make_async_remote_copy(
                src_ref=ref, dst_ref=ref, send_sem=ss.at[k], recv_sem=rs.at[0], device_id={"fs": f, "tp": twin}
            ).wait_send()

    plan, has = broadcast_plan()
    events = []

    def when(time, fn):
        events.append((time, len(events), fn))

    for start, d, s, o in plan:
        when(start, lambda d=d, s=s, o=o: send_piece(d, s, o))

    when(1.5, ag1.start)
    when(1.6, sag.start)
    for k, time in ((0, 5.5), (3, 5.5), (1, 8.5), (2, 8.5), (4, 11.0), (5, 11.0)):
        when(time, lambda k=k: ag1.got(k))
        when(time + 0.01, lambda k=k: sag.got(k))

    def twin1():
        for k in range(8):
            ag1.got_twin(k)
            sag.got_twin(k)

    when(13.0, twin1)
    for b in range(8):
        when(13.2 + 0.6 * b, lambda b=b: norm1(b))
    when(18.2, finish_norm)

    p_done = max(has[0].values())

    def pool_ring():
        for o in has[0]:
            ensure(0, o)
        pag.start()

    when(p_done, pool_ring)
    for k, time in ((0, 8.5), (3, 8.5), (1, 14.5), (2, 14.5), (4, 20.5), (5, 20.5)):
        when(p_done + time, lambda k=k: pag.got(k))

    def twin_pool():
        for k in range(8):
            pag.got_twin(k)

    when(p_done + 24.0, twin_pool)
    for b in range(8):
        when(p_done + 24.5 + b, lambda b=b: unpack_in(b))
        when(p_done + 25.0 + b, lambda b=b: unpack_out(b))

    g_done = max(max(has[s].values()) for s in PIECES_G)

    def gates():
        for s in PIECES_G:
            for o in has[s]:
                ensure(s, o)

    when(g_done, gates)
    for j in range(6):
        when(g_done + 0.1 + 1.5 * j, lambda j=j: hidden(j))

    def plane(oz):
        for s in PIECES_D:
            for oy in range(NY):
                ensure(s, (oz, oy))
        unpack_down((z - oz + NZ) % NZ)

    def clear_down():
        dfull[:, FB:768, :] = jnp.zeros((8, 768 - FB, BLK), BF)

    when(0.5, clear_down)
    for oz in range(NZ):
        when(max(has[s][oz, oy] for s in PIECES_D for oy in range(NY)), lambda oz=oz: plane(oz))

    for _, _, fn in sorted(events, key=lambda e: e[:2]):
        fn()

    summed_down(snd1, pre1, sr1, rr1, r1s, r1r)
    xall2[t] = (stream[...].astype(F32) + 0.5 * (mine[0] * dsc[...])).astype(BF)
    ag2.start()
    for k in (0, 3, 1, 2, 4, 5):
        ag2.got(k)
    for k in (6, 7, 0, 3, 1, 2, 4, 5):
        ag2.got_twin(k)

    for b in range(8):
        v = norm_block(b, xall2, gainm, b == 0)
        part = jnp.dot(v, infull[b * BLK : (b + 1) * BLK, :], preferred_element_type=F32)
        pacc[...] = part if b == 0 else pacc[...] + part
    finish_norm()
    row = lax.broadcasted_iota(jnp.int32, (SEQ, SEQ), 0)
    col = lax.broadcasted_iota(jnp.int32, (SEQ, SEQ), 1)
    for g, window in enumerate(WINDOWS):
        low = jnp.maximum(row - window // 2, 0)
        high = jnp.minimum(row + window - window // 2, SEQ)
        band = jnp.where((col >= low) & (col < high), 1.0, 0.0).astype(BF)
        count = (high - low).astype(F32)
        scale = jnp.concatenate([sall[2 * g, 0:1, 256:320], sall[2 * g + 1, 0:1, 256:320]], axis=1)
        cols = slice(128 * g, 128 * g + 128)
        for q in range(ROWS // SEQ):
            rows = slice(SEQ * q, SEQ * q + SEQ)
            value = (pacc[rows, cols] * rst[rows, :] * scale).astype(BF)
            total = jnp.dot(band, value, preferred_element_type=F32)
            pooled[rows, cols] = (total / count - value.astype(F32)).astype(BF)
    for b in range(8):
        cols = slice(b * BLK, (b + 1) * BLK)
        mix = jnp.dot(pooled[...], outfull[:, cols], preferred_element_type=F32)
        v = (xall2[b].astype(F32) + mix * sall[b, 0:1, 0:256]).astype(BF)
        ambuf[b] = v
        nbuf[:, cols] = norm_block(b, ambuf, gain2, b == 0)
    finish_norm()

    for j in range(6):
        hidden(j)
    summed_down(snd2, pre2, sr2, rr2, r2s, r2r)
    out[...] = (ambuf[t].astype(F32) + 0.5 * (mine[0] * dsc[...])).astype(BF)

    for ref, k in ((pall.at[0, pl.ds(0, 31 * 64), :], 0), (gbuf.at[pl.ds(0, 124 * 16), :], 1), (dbuf.at[pl.ds(0, 62 * 176), :], 2)):
        pltpu.make_async_remote_copy(
            src_ref=ref, dst_ref=ref, send_sem=psend.at[k], recv_sem=precv.at[0, 0], device_id={"fs": neighbour[0], "tp": t}
        ).wait_send()
    for ring in (ag1, sag, pag, ag2):
        ring.done()
    summed_done(snd1, sr1, r1s, r1r)
    summed_done(snd2, sr2, r2s, r2r)


def body(
    stream, gain_first, gain_mixer, gain_second, gate_weight, gate_scale, up_weight, up_scale,
    down_weight, down_scale, pool_in_weight, pool_in_scale, pool_out_weight, pool_out_scale,
):
    def line(v):
        return v.reshape(1, -1)

    vmem = pl.BlockSpec(memory_space=pltpu.VMEM)
    V = pltpu.VMEM
    sem = pltpu.SemaphoreType.DMA
    exchange = [V((4, ROWS, BLK), BF), V((4, ROWS, BLK), BF), V((3, ROWS, BLK), BF), V((3, ROWS, BLK), BF)]
    ring_sems = [sem((2,)), sem((14,))]
    return pl.pallas_call(
        kernel,
        out_shape=jax.ShapeDtypeStruct((ROWS, BLK), BF),
        in_specs=[vmem] * 14,
        out_specs=vmem,
        scratch_shapes=[
            V((D, GUW), BF),
            V((32 * DH, 128), BF),
            V((8, 768, BLK), BF),
            V((8, D, 128), BF),
            V((8, 16, 384), F32),
            V((D, 512), BF),
            V((512, D), BF),
            V((8, ROWS, BLK), BF),
            V((8, ROWS, BLK), BF),
            V((ROWS, D), BF),
            V((8, ROWS, BLK), BF),
            V((ROWS, 768), BF),
            V((ROWS, 128), F32),
            V((ROWS, 128), F32),
            V((ROWS, 512), F32),
            V((ROWS, 512), BF),
            *exchange,
            *exchange,
            V((4, ROWS, BLK), F32),
            sem((3,)), sem((7, 32)),
            *ring_sems, *ring_sems, *ring_sems, *ring_sems,
            sem((2,)), sem((10,)), sem((2,)), sem((10,)),
        ],
        compiler_params=pltpu.CompilerParams(
            collective_id=0, has_side_effects=True, vmem_limit_bytes=60 * 1024 * 1024
        ),
    )(
        stream, line(gain_first), line(gain_mixer), line(gain_second), gate_weight, line(gate_scale), up_weight,
        line(up_scale), down_weight, line(down_scale), pool_in_weight, line(pool_in_scale), pool_out_weight,
        line(pool_out_scale),
    )


def solution(mesh):
    placed = (
        P("fs", "tp"), P(), P(), P(), P("fs", "tp"), P("tp"), P("fs", "tp"), P("tp"), P("tp", "fs"), P("tp"),
        P("fs", "tp"), P("tp"), P("tp", "fs"), P("tp"),
    )
    return jax.shard_map(body, mesh=mesh, in_specs=placed, out_specs=P("fs", "tp"), check_vma=False)
```

time: 302 us -> 116 us (0.38)
  blocking collectives: 149 us -> 0 us
  Pallas kernels: 0 us -> 111 us
  waiting for transfers between devices: 80.2 us -> 0 us
  matrix products: 25.8 us -> 0 us
  starting transfers between devices: 19.3 us -> 0 us
  between operations: 13.7 us -> 0.01 us
  other arithmetic: 7.36 us -> 0 us
    all_to_all x5 -> x0, blocking collectives: 112 us -> none  [the longest x3 61.5 us: from_everyone(): return lax.all_to_all(copies, axis, split_axis=0, concat_axis=0, tiled=True)]
    pallas_call x0 -> x1, Pallas kernels: none -> 111 us  [body(): pl.pallas_call(kernel, out_shape=jax.ShapeDtypeStruct((ROWS, BLK), BF), i...]
    all_gather x1 -> x0, waiting for transfers between devices: 76.1 us -> none  [gather_turned(): whole, at, done = (lax.all_gather(both, axis, axis=0, tiled=True), 0, [])]
    all_gather x1 -> x0, blocking collectives: 37.7 us -> none  [gather_turned(): whole, at, done = (lax.all_gather(both, axis, axis=0, tiled=True), 0, [])]
    dot_general x6 -> x0, matrix products: 25.8 us -> none  [the longest x2 15.5 us: feed_forward(): return jnp.dot(hidden, down_whole, preferred_element_type=jnp.float32)]
    all_to_all x2 -> x0, starting transfers between devices: 19.3 us -> none  [the longest x1 14.6 us: body(): lax.all_to_all(out_whole, 'tp', split_axis=1, concat_axis=0, tiled=True)]
    convert_element_type x14 -> x0, other arithmetic: 4.37 us -> none  [the longest x3 1.26 us: normed(): return (scaled * norm_gain).astype(jnp.bfloat16)]
    all_to_all x2 -> x0, waiting for transfers between devices: 4.13 us -> none  [the longest x1 4.13 us: body(): lax.all_to_all(out_whole, 'tp', split_axis=1, concat_axis=0, tiled=True)]
  transfers between devices with their start and end apart: 3 -> 0, of which waited for: 2 -> 0; matrix products, arithmetic and copies ran while one was open for 1% -> 0% of each run, Pallas kernels for 0% -> 0%
where the time goes in v1:
time: 116 us
  Pallas kernels  111 us (96%)
  local copies, waits for them, and re-layouts  5.31 us (5%)
    pallas_call x1, Pallas kernels, body(): pl.pallas_call(kernel, out_shape=jax.ShapeDtypeStruct((ROWS, BLK), BF), i...  111 us
    unnamed x6, local copies, waits for them, and re-layouts  4.13 us

profile of v1, /device:TPU:1, one launch (start us, length us, event | category | flops | bytes accessed | tf_op | source)
XLA Modules:
  0.0 116.2 jit_solution(13805315834758652681)
XLA Ops:
  0.0 0.0 copy-start
  0.0 0.0 copy-start.1
  0.0 0.7 copy-done
  0.7 0.6 reshape.27.gsc
  1.3 0.0 copy-done.1
  1.3 0.6 reshape.28.usc
  1.9 1.8 %copy.15.dw = f32[704,64]{1,0:T(8,128)} copy(f32[704,64]{0,1:T(8,128)} %param.22) | data formatting | bytes 360448 | tf_op args[8]
  3.7 110.8 %shard_map.136 = bf16[384,256]{1,0:T(8,128)(2,1)} custom-call(bf16[384,256]{1,0:T(8,128)(2,1)} %stream.1, f32[1,2048]{1,0:T(1,128)} %bitcast.6, f32[1,2048]{1,0:T(1,128)} %bitcast.7, f32[1,2048]{1,0:T(1,128)} %bitcast.8, f32[64,704]{1,0:T(8,128)} %gw.1, f32[1,704]{1,0:T(1,128)} %reshape.27.gsc, f32[64,704]{1,0:T(8,128)} %uw.1, f32[1,704]{1,0:T(1,128)} %reshape.28.usc, ...), custom_call_target="tpu_custom_call" | custom-call | tf_op jit(solution)/shard_map/pallas_call | solution.py:452
  114.5 1.6 %copy.17 = bf16[384,256]{1,0:T(8,128)(2,1)} copy(bf16[384,256]{1,0:T(8,128)(2,1)} %shard_map.136) | data formatting | bytes 393216
Async XLA Ops:
  0.0 0.7 copy-start
  0.0 1.3 %copy-start.1 = (f32[704]{0:T(1024)S(1)}, f32[704]{0:T(1024)}, u32[]{:S(2)}) copy-start(f32[704]{0:T(1024)} %param.21) | copy-start | bytes 8452

commit v2 on v1

--- a/solution.py
+++ b/solution.py
@@ -22,9 +22,11 @@
 F32 = jnp.float32
 
 SIZES = (0.36, 1, 1, 1, 1, 1, 1)
-CLASSES = (0, 1, 1, 1, 1, 2, 2)
+RANKS = (-1, 0, 0, 0, 0, 1, 1)
 PIECES_G = (1, 2, 3, 4)
 PIECES_D = (5, 6)
+PLAN = (4.0, 345, 1.0)
+G_LATE, D_LATE = 1.0, 0.5
 
 
 def moved(o, d):
@@ -36,7 +38,7 @@
     return (z + (1 if d == 2 else -1)) % NZ, y
 
 
-def broadcast_plan(lag=2.0, seed=43, noise=0.3):
+def broadcast_plan(lag=PLAN[0], seed=PLAN[1], noise=PLAN[2]):
     rng = random.Random(seed)
     count = len(SIZES)
     has = [{(0, 0): 0.0} for _ in range(count)]
@@ -59,7 +61,7 @@
 
         def key(c):
             onward = sum(moved(c[3], e) not in has[c[1]] for e in range(4))
-            return CLASSES[c[1]], -noise * rng.random() * 4 - onward * 0.5 + len(has[c[1]]) * 0.02
+            return RANKS[c[1]] * 1.5 - noise * rng.random() * 4 - onward * 0.5 + len(has[c[1]]) * 0.02
 
         start, s, o, q = min(found, key=key)
         has[s][q] = start + SIZES[s] + lag
@@ -69,11 +71,11 @@
 
 
 def kernel(
-    stream, gain1, gainm, gain2, gw, gsc, uw, usc, dw, dsc, iw, isc, ow, osc,
+    stream, gain1, gainm, gain2, gw, gsc1, uw, usc1, dw, dsc, iw, isc, ow, osc,
     out,
     gbuf, dbuf, dfull, pall, sall, infull, outfull, xall1, xall2, nbuf, ambuf, hid, ssacc, rst, pacc, pooled,
-    snd1, pre1, sr1, rr1, snd2, pre2, sr2, rr2, mine,
-    psend, precv, a1s, a1r, a2s, a2r, pas, par, sas, sar, r1s, r1r, r2s, r2r,
+    snd1, pre1, sr1, rr1, snd2, pre2, sr2, rr2, mine, tot,
+    gsc, usc, psend, precv, a1s, a1r, a2s, a2r, pas, par, sas, sar, r1s, r1r, r2s, r2r,
 ):
     f, t = lax.axis_index("fs"), lax.axis_index("tp")
     z, y = f // NY, f % NY
@@ -101,11 +103,14 @@
         gbuf[prow, 256 * j : 256 * j + 128] = gw[:, 128 * j : 128 * j + 128].astype(BF)
         gbuf[prow, 256 * j + 128 : 256 * j + 256] = uw[:, 128 * j : 128 * j + 128].astype(BF)
     gbuf[prow, 1280:1408] = jnp.concatenate([gw[:, 640:704], uw[:, 640:704]], axis=1).astype(BF)
-    dbuf[pl.ds(pl.multiple_of(f * DH, 32), DH), :] = jnp.concatenate([dw[0:DH, :], dw[DH:FB, :]], axis=1).astype(BF)
+    down_rows = jnp.transpose(dw[...])
+    dbuf[pl.ds(pl.multiple_of(f * DH, 32), DH), :] = jnp.concatenate([down_rows[0:DH, :], down_rows[DH:FB, :]], axis=1).astype(BF)
     xall1[t] = stream[...]
     sall[t] = jnp.concatenate(
         [jnp.broadcast_to(osc[...], (16, 256)), jnp.broadcast_to(isc[...], (16, 64)), jnp.zeros((16, 64), F32)], axis=1
     )
+    gsc[...] = gsc1[...].reshape(1, FB)
+    usc[...] = usc1[...].reshape(1, FB)
     pl.semaphore_wait(barrier, 7)
 
     def piece(s, owner):
@@ -140,12 +145,12 @@
         ).start()
 
     class Ring:
-        def __init__(self, part, whole, ssem, rsem):
-            self.part, self.whole, self.ssem, self.rsem = part, whole, ssem, rsem
+        def __init__(self, part, whole, ssem, rsem, base=0):
+            self.part, self.whole, self.ssem, self.rsem, self.base = part, whole, ssem, rsem, base
 
         def copy(self, ref, to, rs):
             return pltpu.make_async_remote_copy(
-                src_ref=ref, dst_ref=ref, send_sem=self.ssem.at[1 if rs >= 6 else 0], recv_sem=self.rsem.at[rs],
+                src_ref=ref, dst_ref=ref, send_sem=self.ssem.at[1 if rs >= 6 else 0], recv_sem=self.rsem.at[self.base + rs],
                 device_id={"fs": f, "tp": to},
             )
 
@@ -192,7 +197,6 @@
         )
 
     ag1 = Ring(*halves(xall1, ROWS), a1s, a1r)
-    ag2 = Ring(*halves(xall2, ROWS), a2s, a2r)
     pag = Ring(*halves(pall, D), pas, par)
     sag = Ring(*halves(sall, 16), sas, sar)
     sag.part = lambda b, h: sall.at[b, pl.ds(h * 8, 8), :]
@@ -211,29 +215,31 @@
     def norm1(b):
         nbuf[:, b * BLK : (b + 1) * BLK] = norm_block(b, xall1, gain1, b == 0)
 
-    def hidden(j):
+    def hidden(j, at=0, size=ROWS):
+        rows = slice(at, at + size)
+        r = rst[rows, :]
         if j < 5:
-            acc = jnp.dot(nbuf[...], gbuf[:, 256 * j : 256 * j + 256], preferred_element_type=F32)
-            r = rst[...]
+            acc = jnp.dot(nbuf[rows, :], gbuf[:, 256 * j : 256 * j + 256], preferred_element_type=F32)
             g = acc[:, :128] * r * gsc[:, 128 * j : 128 * j + 128]
             u = acc[:, 128:] * r * usc[:, 128 * j : 128 * j + 128]
-            hid[:, 128 * j : 128 * j + 128] = (g / (1.0 + jnp.exp(-g)) * u).astype(BF)
+            hid[rows, 128 * j : 128 * j + 128] = (g / (1.0 + jnp.exp(-g)) * u).astype(BF)
         else:
-            acc = jnp.dot(nbuf[...], gbuf[:, 1280:1408], preferred_element_type=F32)
+            acc = jnp.dot(nbuf[rows, :], gbuf[:, 1280:1408], preferred_element_type=F32)
             scale = jnp.concatenate([gsc[:, 640:704], usc[:, 640:704]], axis=1)
-            v = acc * rst[...] * scale
+            v = acc * r * scale
             u = pltpu.roll(v, 64, 1)
             h = v / (1.0 + jnp.exp(-v)) * u
             lane = lax.broadcasted_iota(jnp.int32, h.shape, 1)
-            hid[:, 640:768] = jnp.where(lane < 64, h, 0.0).astype(BF)
+            hid[rows, 640:768] = jnp.where(lane < 64, h, 0.0).astype(BF)
 
     def unpack_down(b):
+        side = (b + c) % 2
         for pair in range(2):
             one = dbuf[pl.ds(pl.multiple_of((4 * b + 2 * pair) * DH, 32), DH), :]
             two = dbuf[pl.ds(pl.multiple_of((4 * b + 2 * pair + 1) * DH, 32), DH), :]
-            cols = slice(128 * pair, 128 * pair + 128)
-            dfull[b, 0:DH, cols] = jnp.concatenate([one[:, :64], two[:, :64]], axis=1)
-            dfull[b, DH:FB, cols] = jnp.concatenate([one[:, 64:], two[:, 64:]], axis=1)
+            cols = pl.ds(pl.multiple_of(side * BLK + 128 * pair, 128), 128)
+            dfull[b // 2, 0:DH, cols] = jnp.concatenate([one[:, :64], two[:, :64]], axis=1)
+            dfull[b // 2, DH:FB, cols] = jnp.concatenate([one[:, 64:], two[:, 64:]], axis=1)
 
     def unpack_in(k):
         rows = pl.ds(256 * k, 256)
@@ -248,72 +254,80 @@
                 [pall[b, 128 * i : 128 * i + 64, :][:, 64:], pall[b, 128 * i + 64 : 128 * i + 128, :][:, 64:]], axis=1
             )
 
-    def down(b):
-        return jnp.dot(hid[...], dfull[b], preferred_element_type=F32)
-
-    def summed_down(snd, pre, sr, rr, ss, rs):
-        offs = (0, 1, 2, -1)
-        A, B = pl.ds(0, HALF), pl.ds(HALF, HALF)
-
-        def to_twin(k):
-            snd[k] = down(at_t(offs[k], oc)).astype(BF)
-            pltpu.make_async_remote_copy(
-                src_ref=snd.at[k], dst_ref=pre.at[k], send_sem=ss.at[0], recv_sem=rs.at[k],
+    def down(chip, cols):
+        return jnp.dot(hid[...], dfull[chip, :, cols], preferred_element_type=F32)
+
+    OWN, OTHER = slice(0, BLK), slice(BLK, 2 * BLK)
+
+    SEQS = range(ROWS // SEQ)
+
+    class Sum:
+        def __init__(self, snd, pre, sr, rr, ss, rs):
+            self.snd, self.pre, self.sr, self.rr, self.ss, self.rs = snd, pre, sr, rr, ss, rs
+
+        def pair(self, k):
+            return pltpu.make_async_remote_copy(
+                src_ref=self.snd.at[k], dst_ref=self.pre.at[k], send_sem=self.ss.at[0], recv_sem=self.rs.at[k],
                 device_id={"fs": f, "tp": twin},
-            ).start()
-
-        def own(k):
-            mine[k] = down(at_t(offs[k], c))
-
-        def both(k):
-            pltpu.make_async_remote_copy(
-                src_ref=snd.at[k], dst_ref=pre.at[k], send_sem=ss.at[0], recv_sem=rs.at[k],
-                device_id={"fs": f, "tp": twin},
-            ).wait_recv()
-
-        def hop(src, slot, rows, sem, to):
+            )
+
+        def half(self, q, h):
+            return pl.ds(SEQ * q + h * (SEQ // 2), SEQ // 2)
+
+        def hop(self, q, src, slot, h, sem, to):
+            rows = self.half(q, h)
             return pltpu.make_async_remote_copy(
-                src_ref=src, dst_ref=rr.at[slot, rows, :], send_sem=ss.at[1], recv_sem=rs.at[sem],
-                device_id={"fs": f, "tp": to},
+                src_ref=self.sr.at[src, rows, :], dst_ref=self.rr.at[slot, rows, :], send_sem=self.ss.at[1],
+                recv_sem=self.rs.at[4 + 6 * q + sem], device_id={"fs": f, "tp": to},
             )
 
-        to_twin(2)
-        to_twin(1)
-        own(2)
-        both(2)
-        sr[2] = (mine[2] + pre[2].astype(F32)).astype(BF)
-        hop(sr.at[2, A, :], 2, A, 4, right).start()
-        hop(sr.at[2, B, :], 2, B, 5, left).start()
-        to_twin(3)
-        own(1)
-        both(1)
-        sr[1, B, :] = (mine[1, B, :] + pre[1, B, :].astype(F32)).astype(BF)
-        hop(sr.at[1, B, :], 0, B, 6, right).start()
-        own(3)
-        both(3)
-        sr[0, A, :] = (mine[3, A, :] + pre[3, A, :].astype(F32)).astype(BF)
-        hop(sr.at[0, A, :], 1, A, 7, left).start()
-        to_twin(0)
-        own(0)
-        hop(sr.at[2, A, :], 2, A, 4, right).wait_recv()
-        sr[1, A, :] = (mine[1, A, :] + pre[1, A, :].astype(F32) + rr[2, A, :].astype(F32)).astype(BF)
-        hop(sr.at[1, A, :], 0, A, 8, right).start()
-        hop(sr.at[2, B, :], 2, B, 5, left).wait_recv()
-        sr[0, B, :] = (mine[3, B, :] + pre[3, B, :].astype(F32) + rr[2, B, :].astype(F32)).astype(BF)
-        hop(sr.at[0, B, :], 1, B, 9, left).start()
-        both(0)
-        mine[0] = mine[0] + pre[0].astype(F32)
-        hop(sr.at[1, B, :], 0, B, 6, right).wait_recv()
-        hop(sr.at[0, A, :], 1, A, 7, left).wait_recv()
-        hop(sr.at[1, A, :], 0, A, 8, right).wait_recv()
-        hop(sr.at[0, B, :], 1, B, 9, left).wait_recv()
-        mine[0] = mine[0] + rr[0].astype(F32) + rr[1].astype(F32)
-
-    def summed_done(snd, sr, ss, rs):
-        for ref, k in ((snd.at[pl.ds(0, 4)], 0), (sr.at[pl.ds(0, 3)], 1)):
-            pltpu.make_async_remote_copy(
-                src_ref=ref, dst_ref=ref, send_sem=ss.at[k], recv_sem=rs.at[0], device_id={"fs": f, "tp": twin}
-            ).wait_send()
+        def far(self, total):
+            self.sr[2] = total.astype(BF)
+            for q in SEQS:
+                self.hop(q, 2, 2, 0, 0, right).start()
+                self.hop(q, 2, 2, 1, 1, left).start()
+
+        def near_right(self, total):
+            tot[1] = total
+            for q in SEQS:
+                rows = self.half(q, 1)
+                self.sr[1, rows, :] = tot[1, rows, :].astype(BF)
+                self.hop(q, 1, 0, 1, 2, right).start()
+
+        def near_left(self, total):
+            tot[3] = total
+            for q in SEQS:
+                rows = self.half(q, 0)
+                self.sr[0, rows, :] = tot[3, rows, :].astype(BF)
+                self.hop(q, 0, 1, 0, 3, left).start()
+
+        def through(self, q):
+            rows = self.half(q, 0)
+            self.hop(q, 2, 2, 0, 0, right).wait_recv()
+            self.sr[1, rows, :] = (tot[1, rows, :] + self.rr[2, rows, :].astype(F32)).astype(BF)
+            self.hop(q, 1, 0, 0, 4, right).start()
+            rows = self.half(q, 1)
+            self.hop(q, 2, 2, 1, 1, left).wait_recv()
+            self.sr[0, rows, :] = (tot[3, rows, :] + self.rr[2, rows, :].astype(F32)).astype(BF)
+            self.hop(q, 0, 1, 1, 5, left).start()
+
+        def total(self, q):
+            self.hop(q, 1, 0, 1, 2, right).wait_recv()
+            self.hop(q, 0, 1, 0, 3, left).wait_recv()
+            self.hop(q, 1, 0, 0, 4, right).wait_recv()
+            self.hop(q, 0, 1, 1, 5, left).wait_recv()
+            rows = pl.ds(SEQ * q, SEQ)
+            return tot[0, rows, :] + self.rr[0, rows, :].astype(F32) + self.rr[1, rows, :].astype(F32)
+
+        def done(self):
+            for ref, k in ((self.snd.at[pl.ds(0, 4)], 0), (self.sr.at[pl.ds(0, 3)], 1)):
+                pltpu.make_async_remote_copy(
+                    src_ref=ref, dst_ref=ref, send_sem=self.ss.at[k], recv_sem=self.rs.at[0],
+                    device_id={"fs": f, "tp": twin},
+                ).wait_send()
+
+    first = Sum(snd1, pre1, sr1, rr1, r1s, r1r)
+    second = Sum(snd2, pre2, sr2, rr2, r2s, r2r)
 
     plan, has = broadcast_plan()
     events = []
@@ -348,17 +362,17 @@
         pag.start()
 
     when(p_done, pool_ring)
-    for k, time in ((0, 8.5), (3, 8.5), (1, 14.5), (2, 14.5), (4, 20.5), (5, 20.5)):
+    for k, time in ((0, 8.5), (3, 8.5), (1, 15.0), (2, 15.0), (4, 22.5), (5, 22.5)):
         when(p_done + time, lambda k=k: pag.got(k))
 
     def twin_pool():
         for k in range(8):
             pag.got_twin(k)
 
-    when(p_done + 24.0, twin_pool)
+    when(70.0, twin_pool)
     for b in range(8):
-        when(p_done + 24.5 + b, lambda b=b: unpack_in(b))
-        when(p_done + 25.0 + b, lambda b=b: unpack_out(b))
+        when(70.1, lambda b=b: unpack_in(b))
+        when(70.2, lambda b=b: unpack_out(b))
 
     g_done = max(max(has[s].values()) for s in PIECES_G)
 
@@ -367,9 +381,14 @@
             for o in has[s]:
                 ensure(s, o)
 
-    when(g_done, gates)
-    for j in range(6):
-        when(g_done + 0.1 + 1.5 * j, lambda j=j: hidden(j))
+    when(g_done + G_LATE, gates)
+
+    def hidden_part(js):
+        for j in js:
+            hidden(j)
+
+    when(g_done + G_LATE + 0.1, lambda: hidden_part((0, 1, 2)))
+    when(g_done + G_LATE + 1.9, lambda: hidden_part((3, 4, 5)))
 
     def plane(oz):
         for s in PIECES_D:
@@ -378,27 +397,104 @@
         unpack_down((z - oz + NZ) % NZ)
 
     def clear_down():
-        dfull[:, FB:768, :] = jnp.zeros((8, 768 - FB, BLK), BF)
+        dfull[:, FB:768, :] = jnp.zeros((NX, 768 - FB, 2 * BLK), BF)
 
     when(0.5, clear_down)
+    ready = {oz: max(has[s][oz, oy] for s in PIECES_D for oy in range(NY)) for oz in range(NZ)}
+    even, odd = (sorted(range(e, NZ, 2), key=lambda oz: ready[oz]) for e in (0, 1))
+    turn = (z + c) % 2
+
+    def products(i):
+        one, two = (z - even[i] + NZ) % NZ, (z - odd[i] + NZ) % NZ
+        for_twin = one * turn + two * (1 - turn)
+        own = two * turn + one * (1 - turn)
+        snd1[i] = down(for_twin // 2, OTHER).astype(BF)
+        first.pair(i).start()
+        mine[i] = down(own // 2, OWN)
+
+    def combine(i):
+        one, two = (z - even[i] + NZ) % NZ, (z - odd[i] + NZ) % NZ
+        own = two * turn + one * (1 - turn)
+        away = (own // 2 - x + NX) % NX
+        first.pair(i).wait_recv()
+        mine[i] = mine[i] + pre1[i].astype(F32)
+
+        @pl.when(away == 2)
+        def _():
+            first.far(mine[i])
+
+        @pl.when(away == 1)
+        def _():
+            first.near_right(mine[i])
+
+        @pl.when(away == 3)
+        def _():
+            first.near_left(mine[i])
+
+        @pl.when(away == 0)
+        def _():
+            tot[0] = mine[i]
+
+    hid_done = g_done + G_LATE + 3.6
     for oz in range(NZ):
-        when(max(has[s][oz, oy] for s in PIECES_D for oy in range(NY)), lambda oz=oz: plane(oz))
+        when(ready[oz] + D_LATE, lambda oz=oz: plane(oz))
+    for i in range(4):
+        at = max(hid_done + 1.0 * i, max(ready[even[i]], ready[odd[i]]) + D_LATE + 0.01)
+        when(at, lambda i=i: products(i))
+        when(at + 1.6, lambda i=i: combine(i))
 
     for _, _, fn in sorted(events, key=lambda e: e[:2]):
         fn()
 
-    summed_down(snd1, pre1, sr1, rr1, r1s, r1r)
-    xall2[t] = (stream[...].astype(F32) + 0.5 * (mine[0] * dsc[...])).astype(BF)
-    ag2.start()
-    for k in (0, 3, 1, 2, 4, 5):
-        ag2.got(k)
-    for k in (6, 7, 0, 3, 1, 2, 4, 5):
-        ag2.got_twin(k)
-
-    for b in range(8):
-        v = norm_block(b, xall2, gainm, b == 0)
-        part = jnp.dot(v, infull[b * BLK : (b + 1) * BLK, :], preferred_element_type=F32)
-        pacc[...] = part if b == 0 else pacc[...] + part
+    for q in SEQS:
+        first.through(q)
+    gathers = []
+    for q in SEQS:
+        gather = Ring(
+            lambda b, h, q=q: xall2.at[b, pl.ds(SEQ * q + h * (SEQ // 2), SEQ // 2), :],
+            lambda n: xall2.at[pl.ds(0, n)], a2s, a2r, 14 * q,
+        )
+        gathers.append(gather)
+        rows = pl.ds(SEQ * q, SEQ)
+        xall2[t, rows, :] = (stream[rows, :].astype(F32) + 0.5 * (first.total(q) * dsc[...])).astype(BF)
+        gather.start()
+
+    def enter(b, start=False):
+        v = xall2[b].astype(F32)
+        sq = v * v
+        sq = sq[:, :128] + sq[:, 128:]
+        at = pl.multiple_of(b * BLK, BLK)
+        w = (v * gainm[:, pl.ds(at, BLK)]).astype(BF)
+        part = jnp.dot(w, infull[pl.ds(at, BLK), :], preferred_element_type=F32)
+        ssacc[...] = sq if start else ssacc[...] + sq
+        pacc[...] = part if start else pacc[...] + part
+
+    enter(t, True)
+    for q in SEQS:
+        for k in (0, 3):
+            gathers[q].got(k)
+    for q in SEQS:
+        gathers[q].got_twin(6)
+        gathers[q].got_twin(7)
+    enter(twin)
+    for q in SEQS:
+        for k in (1, 2):
+            gathers[q].got(k)
+    enter(left)
+    enter(right)
+    for q in SEQS:
+        for k in (0, 1, 2, 3):
+            gathers[q].got_twin(k)
+    enter(at_t(-1, oc))
+    enter(at_t(1, oc))
+    for q in SEQS:
+        for k in (4, 5):
+            gathers[q].got(k)
+    enter(at_t(2, c))
+    for q in SEQS:
+        for k in (4, 5):
+            gathers[q].got_twin(k)
+    enter(at_t(2, oc))
     finish_norm()
     row = lax.broadcasted_iota(jnp.int32, (SEQ, SEQ), 0)
     col = lax.broadcasted_iota(jnp.int32, (SEQ, SEQ), 1)
@@ -409,11 +505,11 @@
         count = (high - low).astype(F32)
         scale = jnp.concatenate([sall[2 * g, 0:1, 256:320], sall[2 * g + 1, 0:1, 256:320]], axis=1)
         cols = slice(128 * g, 128 * g + 128)
-        for q in range(ROWS // SEQ):
+        for q in SEQS:
             rows = slice(SEQ * q, SEQ * q + SEQ)
             value = (pacc[rows, cols] * rst[rows, :] * scale).astype(BF)
-            total = jnp.dot(band, value, preferred_element_type=F32)
-            pooled[rows, cols] = (total / count - value.astype(F32)).astype(BF)
+            whole = jnp.dot(band, value, preferred_element_type=F32)
+            pooled[rows, cols] = (whole / count - value.astype(F32)).astype(BF)
     for b in range(8):
         cols = slice(b * BLK, (b + 1) * BLK)
         mix = jnp.dot(pooled[...], outfull[:, cols], preferred_element_type=F32)
@@ -424,17 +520,40 @@
 
     for j in range(6):
         hidden(j)
-    summed_down(snd2, pre2, sr2, rr2, r2s, r2r)
-    out[...] = (ambuf[t].astype(F32) + 0.5 * (mine[0] * dsc[...])).astype(BF)
+
+    def products2(k):
+        chip = (x + (0, 1, 2, -1)[k] + NX) % NX
+        res = down(chip, slice(0, 2 * BLK))
+        snd2[k] = res[:, OTHER].astype(BF)
+        second.pair(k).start()
+        mine[k] = res[:, OWN]
+
+    def both(k):
+        second.pair(k).wait_recv()
+        return mine[k] + pre2[k].astype(F32)
+
+    products2(2)
+    products2(1)
+    second.far(both(2))
+    products2(3)
+    second.near_right(both(1))
+    products2(0)
+    second.near_left(both(3))
+    tot[0] = both(0)
+    for q in SEQS:
+        second.through(q)
+    for q in SEQS:
+        rows = pl.ds(SEQ * q, SEQ)
+        out[rows, :] = (ambuf[t, rows, :].astype(F32) + 0.5 * (second.total(q) * dsc[...])).astype(BF)
 
     for ref, k in ((pall.at[0, pl.ds(0, 31 * 64), :], 0), (gbuf.at[pl.ds(0, 124 * 16), :], 1), (dbuf.at[pl.ds(0, 62 * 176), :], 2)):
         pltpu.make_async_remote_copy(
             src_ref=ref, dst_ref=ref, send_sem=psend.at[k], recv_sem=precv.at[0, 0], device_id={"fs": neighbour[0], "tp": t}
         ).wait_send()
-    for ring in (ag1, sag, pag, ag2):
+    for ring in (ag1, sag, pag, gather):
         ring.done()
-    summed_done(snd1, sr1, r1s, r1r)
-    summed_done(snd2, sr2, r2s, r2r)
+    first.done()
+    second.done()
 
 
 def body(
@@ -457,7 +576,7 @@
         scratch_shapes=[
             V((D, GUW), BF),
             V((32 * DH, 128), BF),
-            V((8, 768, BLK), BF),
+            V((NX, 768, 2 * BLK), BF),
             V((8, D, 128), BF),
             V((8, 16, 384), F32),
             V((D, 512), BF),
@@ -474,16 +593,18 @@
             *exchange,
             *exchange,
             V((4, ROWS, BLK), F32),
+            V((4, ROWS, BLK), F32),
+            V((1, FB), F32), V((1, FB), F32),
             sem((3,)), sem((7, 32)),
-            *ring_sems, *ring_sems, *ring_sems, *ring_sems,
-            sem((2,)), sem((10,)), sem((2,)), sem((10,)),
+            *ring_sems, sem((2,)), sem((42,)), *ring_sems, *ring_sems,
+            sem((2,)), sem((22,)), sem((2,)), sem((22,)),
         ],
         compiler_params=pltpu.CompilerParams(
             collective_id=0, has_side_effects=True, vmem_limit_bytes=60 * 1024 * 1024
         ),
     )(
-        stream, line(gain_first), line(gain_mixer), line(gain_second), gate_weight, line(gate_scale), up_weight,
-        line(up_scale), down_weight, line(down_scale), pool_in_weight, line(pool_in_scale), pool_out_weight,
+        stream, line(gain_first), line(gain_mixer), line(gain_second), gate_weight, gate_scale, up_weight,
+        up_scale, down_weight.T, line(down_scale), pool_in_weight, line(pool_in_scale), pool_out_weight,
         line(pool_out_scale),
     )
 

time: 116 us -> 102 us (0.88)
  Pallas kernels: 111 us -> 100 us
  local copies, waits for them, and re-layouts: 5.31 us -> 1.62 us
    pallas_call x1, Pallas kernels: 111 us -> 100 us  [body(): pl.pallas_call(kernel, out_shape=jax.ShapeDtypeStruct((ROWS, BLK), BF), i...]
    unnamed x6 -> x1, local copies, waits for them, and re-layouts: 4.13 us -> 1.62 us
    reshape x2 -> x0, local copies, waits for them, and re-layouts: 1.18 us -> none  [line(): return v.reshape(1, -1)]
where the time goes in v2:
time: 102 us
  Pallas kernels  100 us (98%)
  local copies, waits for them, and re-layouts  1.62 us (2%)
    pallas_call x1, Pallas kernels, body(): pl.pallas_call(kernel, out_shape=jax.ShapeDtypeStruct((ROWS, BLK), BF), i...  100 us

profile of v2, /device:TPU:1, one launch (start us, length us, event | category | flops | bytes accessed | tf_op | source)
XLA Modules:
  0.0 101.6 jit_solution(16061541854667065652)
XLA Ops:
  0.0 100.0 %shard_map.136 = bf16[384,256]{1,0:T(8,128)(2,1)} custom-call(bf16[384,256]{1,0:T(8,128)(2,1)} %stream.1, f32[1,2048]{1,0:T(1,128)} %bitcast.8, f32[1,2048]{1,0:T(1,128)} %bitcast.9, f32[1,2048]{1,0:T(1,128)} %bitcast.10, f32[64,704]{1,0:T(8,128)} %gw.1, f32[704]{0:T(1024)} %gsc1.1, f32[64,704]{1,0:T(8,128)} %uw.1, f32[704]{0:T(1024)} %usc1.1, ...), custom_call_target="tpu_custom_call" | custom-call | tf_op jit(solution)/shard_map/pallas_call | solution.py:571
  100.0 1.6 %copy.16 = bf16[384,256]{1,0:T(8,128)(2,1)} copy(bf16[384,256]{1,0:T(8,128)(2,1)} %shard_map.136) | data formatting | bytes 393216

commit v3 on v2

--- a/solution.py
+++ b/solution.py
@@ -25,7 +25,7 @@
 RANKS = (-1, 0, 0, 0, 0, 1, 1)
 PIECES_G = (1, 2, 3, 4)
 PIECES_D = (5, 6)
-PLAN = (4.0, 345, 1.0)
+PLAN = (4.0, 10186, 1.0)
 G_LATE, D_LATE = 1.0, 0.5
 
 
@@ -369,10 +369,6 @@
         for k in range(8):
             pag.got_twin(k)
 
-    when(70.0, twin_pool)
-    for b in range(8):
-        when(70.1, lambda b=b: unpack_in(b))
-        when(70.2, lambda b=b: unpack_out(b))
 
     g_done = max(max(has[s].values()) for s in PIECES_G)
 
@@ -408,9 +404,10 @@
         one, two = (z - even[i] + NZ) % NZ, (z - odd[i] + NZ) % NZ
         for_twin = one * turn + two * (1 - turn)
         own = two * turn + one * (1 - turn)
-        snd1[i] = down(for_twin // 2, OTHER).astype(BF)
+        theirs, ours = down(for_twin // 2, OTHER), down(own // 2, OWN)
+        snd1[i] = theirs.astype(BF)
+        mine[i] = ours
         first.pair(i).start()
-        mine[i] = down(own // 2, OWN)
 
     def combine(i):
         one, two = (z - even[i] + NZ) % NZ, (z - odd[i] + NZ) % NZ
@@ -442,6 +439,14 @@
         at = max(hid_done + 1.0 * i, max(ready[even[i]], ready[odd[i]]) + D_LATE + 0.01)
         when(at, lambda i=i: products(i))
         when(at + 1.6, lambda i=i: combine(i))
+
+    def pool_weights():
+        twin_pool()
+        for b in range(8):
+            unpack_in(b)
+            unpack_out(b)
+
+    when(at + 0.2, pool_weights)
 
     for _, _, fn in sorted(events, key=lambda e: e[:2]):
         fn()
@@ -505,11 +510,13 @@
         count = (high - low).astype(F32)
         scale = jnp.concatenate([sall[2 * g, 0:1, 256:320], sall[2 * g + 1, 0:1, 256:320]], axis=1)
         cols = slice(128 * g, 128 * g + 128)
+        value = (pacc[:, cols] * rst[...] * scale).astype(BF)
+        side = jnp.concatenate([value[SEQ * q : SEQ * q + SEQ] for q in SEQS], axis=1)
+        whole = jnp.dot(band, side, preferred_element_type=F32)
         for q in SEQS:
             rows = slice(SEQ * q, SEQ * q + SEQ)
-            value = (pacc[rows, cols] * rst[rows, :] * scale).astype(BF)
-            whole = jnp.dot(band, value, preferred_element_type=F32)
-            pooled[rows, cols] = (whole / count - value.astype(F32)).astype(BF)
+            mean = whole[:, SEQ * q : SEQ * q + SEQ] / count
+            pooled[rows, cols] = (mean - value[rows].astype(F32)).astype(BF)
     for b in range(8):
         cols = slice(b * BLK, (b + 1) * BLK)
         mix = jnp.dot(pooled[...], outfull[:, cols], preferred_element_type=F32)
@@ -534,8 +541,8 @@
 
     products2(2)
     products2(1)
+    products2(3)
     second.far(both(2))
-    products2(3)
     second.near_right(both(1))
     products2(0)
     second.near_left(both(3))

time: 102 us -> 100 us (0.980)
  Pallas kernels: 100 us -> 98.6 us
    pallas_call x1, Pallas kernels: 100 us -> 98.6 us  [body(): pl.pallas_call(kernel, out_shape=jax.ShapeDtypeStruct((ROWS, BLK), BF), i...]
where the time goes in v3:
time: 100 us
  Pallas kernels  98.6 us (99%)
  local copies, waits for them, and re-layouts  1.62 us (2%)
    pallas_call x1, Pallas kernels, body(): pl.pallas_call(kernel, out_shape=jax.ShapeDtypeStruct((ROWS, BLK), BF), i...  98.6 us

profile of v3, /device:TPU:1, one launch (start us, length us, event | category | flops | bytes accessed | tf_op | source)
XLA Modules:
  0.0 100.3 jit_solution(11816423915019607386)
XLA Ops:
  0.0 98.6 %shard_map.136 = bf16[384,256]{1,0:T(8,128)(2,1)} custom-call(bf16[384,256]{1,0:T(8,128)(2,1)} %stream.1, f32[1,2048]{1,0:T(1,128)} %bitcast.8, f32[1,2048]{1,0:T(1,128)} %bitcast.9, f32[1,2048]{1,0:T(1,128)} %bitcast.10, f32[64,704]{1,0:T(8,128)} %gw.1, f32[704]{0:T(1024)} %gsc1.1, f32[64,704]{1,0:T(8,128)} %uw.1, f32[704]{0:T(1024)} %usc1.1, ...), custom_call_target="tpu_custom_call" | custom-call | tf_op jit(solution)/shard_map/pallas_call | solution.py:578
  98.6 1.6 %copy.16 = bf16[384,256]{1,0:T(8,128)(2,1)} copy(bf16[384,256]{1,0:T(8,128)(2,1)} %shard_map.136) | data formatting | bytes 393216

commit v4 on v3

--- a/solution.py
+++ b/solution.py
@@ -71,12 +71,15 @@
 
 
 def kernel(
-    stream, gain1, gainm, gain2, gw, gsc1, uw, usc1, dw, dsc, iw, isc, ow, osc,
-    out,
-    gbuf, dbuf, dfull, pall, sall, infull, outfull, xall1, xall2, nbuf, ambuf, hid, ssacc, rst, pacc, pooled,
-    snd1, pre1, sr1, rr1, snd2, pre2, sr2, rr2, mine, tot,
-    gsc, usc, psend, precv, a1s, a1r, a2s, a2r, pas, par, sas, sar, r1s, r1r, r2s, r2r,
+    *refs,
 ):
+    hbm, out, rest = refs[:14], refs[14], refs[15:]
+    (
+        gbuf, dbuf, dfull, pall, sall, infull, outfull, xall1, xall2, nbuf, ambuf, hid, ssacc, rst, pacc, pooled,
+        snd1, pre1, sr1, rr1, snd2, pre2, sr2, rr2, mine, tot,
+        gsc, usc, psend, precv, a1s, a1r, a2s, a2r, pas, par, sas, sar, r1s, r1r, r2s, r2r,
+        gain1, gainm, gain2, gw, gsc1, uw, usc1, dw, dsc, iw, isc, ow, osc, insem,
+    ) = rest
     f, t = lax.axis_index("fs"), lax.axis_index("tp")
     z, y = f // NY, f % NY
     x, c = t // 2, t % 2
@@ -87,6 +90,15 @@
 
     def at_t(dx, core):
         return ((x + dx + NX) % NX) * 2 + core
+
+    inputs = [
+        pltpu.make_async_copy(src, dst, insem.at[i])
+        for i, (src, dst) in enumerate(
+            zip(hbm, (xall1.at[t], gain1, gainm, gain2, gw, gsc1, uw, usc1, dw, dsc, iw, isc, ow, osc))
+        )
+    ]
+    for i in (10, 12, 4, 6, 8, 0, 1, 2, 3, 5, 7, 9, 11, 13):
+        inputs[i].start()
 
     neighbour = [at_f(0, 1), at_f(0, -1), at_f(1, 0), at_f(-1, 0)]
     right, left, twin = at_t(1, c), at_t(-1, c), at_t(0, oc)
@@ -97,6 +109,8 @@
     for nt in (right, left, twin):
         pl.semaphore_signal(barrier, inc=1, device_id={"fs": f, "tp": nt})
 
+    for copy in inputs:
+        copy.wait()
     prow = pl.ds(pl.multiple_of(f * 64, 64), 64)
     pall[t, prow, :] = jnp.concatenate([iw[...], ow[...]], axis=1).astype(BF)
     for j in range(5):
@@ -105,7 +119,6 @@
     gbuf[prow, 1280:1408] = jnp.concatenate([gw[:, 640:704], uw[:, 640:704]], axis=1).astype(BF)
     down_rows = jnp.transpose(dw[...])
     dbuf[pl.ds(pl.multiple_of(f * DH, 32), DH), :] = jnp.concatenate([down_rows[0:DH, :], down_rows[DH:FB, :]], axis=1).astype(BF)
-    xall1[t] = stream[...]
     sall[t] = jnp.concatenate(
         [jnp.broadcast_to(osc[...], (16, 256)), jnp.broadcast_to(isc[...], (16, 64)), jnp.zeros((16, 64), F32)], axis=1
     )
@@ -461,7 +474,7 @@
         )
         gathers.append(gather)
         rows = pl.ds(SEQ * q, SEQ)
-        xall2[t, rows, :] = (stream[rows, :].astype(F32) + 0.5 * (first.total(q) * dsc[...])).astype(BF)
+        xall2[t, rows, :] = (xall1[t, rows, :].astype(F32) + 0.5 * (first.total(q) * dsc[...])).astype(BF)
         gather.start()
 
     def enter(b, start=False):
@@ -570,6 +583,11 @@
     def line(v):
         return v.reshape(1, -1)
 
+    operands = (
+        stream, line(gain_first), line(gain_mixer), line(gain_second), gate_weight, gate_scale, up_weight,
+        up_scale, down_weight.T, line(down_scale), pool_in_weight, line(pool_in_scale), pool_out_weight,
+        line(pool_out_scale),
+    )
     vmem = pl.BlockSpec(memory_space=pltpu.VMEM)
     V = pltpu.VMEM
     sem = pltpu.SemaphoreType.DMA
@@ -578,7 +596,7 @@
     return pl.pallas_call(
         kernel,
         out_shape=jax.ShapeDtypeStruct((ROWS, BLK), BF),
-        in_specs=[vmem] * 14,
+        in_specs=[pl.BlockSpec(memory_space=pltpu.HBM)] * 14,
         out_specs=vmem,
         scratch_shapes=[
             V((D, GUW), BF),
@@ -605,15 +623,14 @@
             sem((3,)), sem((7, 32)),
             *ring_sems, sem((2,)), sem((42,)), *ring_sems, *ring_sems,
             sem((2,)), sem((22,)), sem((2,)), sem((22,)),
+            V((1, D), F32), V((1, D), F32), V((1, D), F32), V((64, FB), F32), V((FB,), F32), V((64, FB), F32), V((FB,), F32),
+            V((64, FB), F32), V((1, BLK), F32), V((64, 64), F32), V((1, 64), F32), V((64, 64), F32), V((1, BLK), F32),
+            sem((14,)),
         ],
         compiler_params=pltpu.CompilerParams(
-            collective_id=0, has_side_effects=True, vmem_limit_bytes=60 * 1024 * 1024
+            collective_id=0, has_side_effects=True, vmem_limit_bytes=42 * 1024 * 1024
         ),
-    )(
-        stream, line(gain_first), line(gain_mixer), line(gain_second), gate_weight, gate_scale, up_weight,
-        up_scale, down_weight.T, line(down_scale), pool_in_weight, line(pool_in_scale), pool_out_weight,
-        line(pool_out_scale),
-    )
+    )(*(pltpu.with_memory_space_constraint(v, pltpu.HBM) for v in operands))
 
 
 def solution(mesh):

time: 100 us -> 97.5 us (0.975)
  Pallas kernels: 98.6 us -> 96.7 us
    pallas_call x1, Pallas kernels: 98.6 us -> 96.7 us  [body(): pl.pallas_call(kernel, out_shape=jax.ShapeDtypeStruct((ROWS, BLK), BF), i...]
where the time goes in v4:
time: 97.5 us; the launch traced here: 97.4 us
  Pallas kernels  96.7 us (99%)
    pallas_call x1, Pallas kernels, body(): pl.pallas_call(kernel, out_shape=jax.ShapeDtypeStruct((ROWS, BLK), BF), i...  96.7 us

profile of v4, /device:TPU:1, one launch (start us, length us, event | category | flops | bytes accessed | tf_op | source)
XLA Modules:
  0.0 97.4 jit_solution(17243709941651597400)
XLA Ops:
  0.0 96.7 %shard_map.136 = bf16[384,256]{1,0:T(8,128)(2,1)S(1)} custom-call(bf16[384,256]{1,0:T(8,128)(2,1)} %refs_0_.1, f32[1,2048]{1,0:T(1,128)} %bitcast.8, f32[1,2048]{1,0:T(1,128)} %bitcast.9, f32[1,2048]{1,0:T(1,128)} %bitcast.10, f32[64,704]{1,0:T(8,128)} %refs_4_.1, f32[704]{0:T(1024)} %refs_5_.1, f32[64,704]{1,0:T(8,128)} %refs_6_.1, f32[704]{0:T(1024)} %refs_7_.1, ...), custom_call_target="tpu_custom_call" | custom-call | tf_op jit(solution)/shard_map/pallas_call | solution.py:596
  96.7 0.7 copy.16

commit v5 on v4

--- a/solution.py
+++ b/solution.py
@@ -109,22 +109,30 @@
     for nt in (right, left, twin):
         pl.semaphore_signal(barrier, inc=1, device_id={"fs": f, "tp": nt})
 
-    for copy in inputs:
-        copy.wait()
     prow = pl.ds(pl.multiple_of(f * 64, 64), 64)
+    inputs[10].wait()
+    inputs[12].wait()
     pall[t, prow, :] = jnp.concatenate([iw[...], ow[...]], axis=1).astype(BF)
+    inputs[4].wait()
+    inputs[6].wait()
     for j in range(5):
         gbuf[prow, 256 * j : 256 * j + 128] = gw[:, 128 * j : 128 * j + 128].astype(BF)
         gbuf[prow, 256 * j + 128 : 256 * j + 256] = uw[:, 128 * j : 128 * j + 128].astype(BF)
     gbuf[prow, 1280:1408] = jnp.concatenate([gw[:, 640:704], uw[:, 640:704]], axis=1).astype(BF)
-    down_rows = jnp.transpose(dw[...])
-    dbuf[pl.ds(pl.multiple_of(f * DH, 32), DH), :] = jnp.concatenate([down_rows[0:DH, :], down_rows[DH:FB, :]], axis=1).astype(BF)
-    sall[t] = jnp.concatenate(
-        [jnp.broadcast_to(osc[...], (16, 256)), jnp.broadcast_to(isc[...], (16, 64)), jnp.zeros((16, 64), F32)], axis=1
-    )
-    gsc[...] = gsc1[...].reshape(1, FB)
-    usc[...] = usc1[...].reshape(1, FB)
     pl.semaphore_wait(barrier, 7)
+
+    def pack_rest():
+        for i in (8, 0, 1, 2, 3, 5, 7, 9, 11, 13):
+            inputs[i].wait()
+        down_rows = jnp.transpose(dw[...])
+        dbuf[pl.ds(pl.multiple_of(f * DH, 32), DH), :] = jnp.concatenate(
+            [down_rows[0:DH, :], down_rows[DH:FB, :]], axis=1
+        ).astype(BF)
+        sall[t] = jnp.concatenate(
+            [jnp.broadcast_to(osc[...], (16, 256)), jnp.broadcast_to(isc[...], (16, 64)), jnp.zeros((16, 64), F32)], axis=1
+        )
+        gsc[...] = gsc1[...].reshape(1, FB)
+        usc[...] = usc1[...].reshape(1, FB)
 
     def piece(s, owner):
         if s == 0:
@@ -351,6 +359,8 @@
     for start, d, s, o in plan:
         when(start, lambda d=d, s=s, o=o: send_piece(d, s, o))
 
+    first_down = min(start for start, _, s, _ in plan if s in PIECES_D)
+    when(min(0.4, first_down - 1e-3), pack_rest)
     when(1.5, ag1.start)
     when(1.6, sag.start)
     for k, time in ((0, 5.5), (3, 5.5), (1, 8.5), (2, 8.5), (4, 11.0), (5, 11.0)):
@@ -456,7 +466,6 @@
     def pool_weights():
         twin_pool()
         for b in range(8):
-            unpack_in(b)
             unpack_out(b)
 
     when(at + 0.2, pool_weights)
@@ -487,6 +496,8 @@
         ssacc[...] = sq if start else ssacc[...] + sq
         pacc[...] = part if start else pacc[...] + part
 
+    for b in range(8):
+        unpack_in(b)
     enter(t, True)
     for q in SEQS:
         for k in (0, 3):

time: 97.5 us -> 97.6 us (level)
  no operation moved by 1% of the time
where the time goes in v5:
time: 97.6 us; the launch traced here: 97.5 us
  Pallas kernels  96.8 us (99%)
    pallas_call x1, Pallas kernels, body(): pl.pallas_call(kernel, out_shape=jax.ShapeDtypeStruct((ROWS, BLK), BF), i...  96.8 us

profile of v5, /device:TPU:1, one launch (start us, length us, event | category | flops | bytes accessed | tf_op | source)
XLA Modules:
  0.0 97.5 jit_solution(15264036442142583927)
XLA Ops:
  0.0 96.8 %shard_map.136 = bf16[384,256]{1,0:T(8,128)(2,1)S(1)} custom-call(bf16[384,256]{1,0:T(8,128)(2,1)} %refs_0_.1, f32[1,2048]{1,0:T(1,128)} %bitcast.8, f32[1,2048]{1,0:T(1,128)} %bitcast.9, f32[1,2048]{1,0:T(1,128)} %bitcast.10, f32[64,704]{1,0:T(8,128)} %refs_4_.1, f32[704]{0:T(1024)} %refs_5_.1, f32[64,704]{1,0:T(8,128)} %refs_6_.1, f32[704]{0:T(1024)} %refs_7_.1, ...), custom_call_target="tpu_custom_call" | custom-call | tf_op jit(solution)/shard_map/pallas_call | solution.py:607
  96.8 0.7 copy.16
